TPU v7x, 32 devices: a whole 2x2x4 slice. The times are simulated.
32 devices in a mesh: sp: 8 (over z, x), dp: 4 (over y, core).
Axes of the slice: x: 2, y: 2, z: 4, core: 2. Of those that a mesh axis runs over, the one named last changes fastest.
Arguments:
- queries: bfloat16 [4, 1024, 2048], P('dp', 'sp'), may hold values from -6 to 6
- keys: bfloat16 [4, 1024, 2048], P('dp', 'sp'), may hold values from -6 to 6
- values: bfloat16 [4, 1024, 2048], P('dp', 'sp'), may hold values from -6 to 6
- gate_totals: float32 [4, 1024, 32], P('dp', 'sp'), may hold values from -1024 to 0, as said below
- w_out: bfloat16 [2048, 2048], P(None, 'dp'), may hold values from -1 to 1
Outputs:
- mixed: bfloat16 [4, 1024, 2048], P('dp', 'sp')
Inputs may be any that keep to these rules, and one draw needn't show every extreme that they name: `gate_totals`: never rising along a sequence.
All inputs are finite; a program needn't handle non-finite values.
Results may differ from a plain program's by a relative error of at most 0.0053.
Values may be sent and summed in bfloat16 or wider, within the bound.
A program may use at most 64 MiB of HBM per device.

v0:
```python
import jax
import jax.numpy as jnp
from jax import lax
from jax.sharding import PartitionSpec as P

HEAD_DIM = 64


def attend(queries, key_rows, value_rows, totals):
    length = queries.shape[0]
    block_rows = min(length, 512)
    pieces = []
    for begin_row in range(0, length, block_rows):
        end_row = begin_row + block_rows
        scaled = queries[begin_row:end_row] * jnp.bfloat16(HEAD_DIM ** (-0.5))
        scores = jnp.einsum(
            "qhd,khd->hqk", scaled, key_rows[:end_row], preferred_element_type=jnp.float32
        )
        causal = jnp.arange(end_row)[None, :] <= (begin_row + jnp.arange(block_rows))[:, None]
        scores = jnp.where(
            causal[None],
            scores
            + jnp.transpose(totals[begin_row:end_row])[:, :, None]
            - jnp.transpose(totals[:end_row])[:, None, :],
            -jnp.inf,
        )
        biggest = jnp.max(scores, axis=-1, keepdims=True)
        expo = jnp.exp(scores - biggest)
        summed = jnp.sum(expo, axis=-1)
        weights = expo.astype(jnp.bfloat16)
        output = jnp.einsum(
            "hqk,khd->qhd", weights, value_rows[:end_row], preferred_element_type=jnp.float32
        )
        output = output / jnp.transpose(summed)[:, :, None]
        pieces.append(output.astype(jnp.bfloat16))
    return jnp.concatenate(pieces, axis=0).reshape(length, -1)


def local(queries, keys, values, gate_totals, w_out):
    moved = (
        lax.all_to_all(queries, "sp", split_axis=2, concat_axis=1, tiled=True),
        lax.all_to_all(keys, "sp", split_axis=2, concat_axis=1, tiled=True),
        lax.all_to_all(values, "sp", split_axis=2, concat_axis=1, tiled=True),
    )
    totals = lax.all_to_all(gate_totals, "sp", split_axis=2, concat_axis=1, tiled=True)
    held, length = (moved[0].shape[0], moved[0].shape[1])
    query_heads, key_heads, value_heads = [
        part_array[0].reshape(length, -1, HEAD_DIM) for part_array in moved
    ]
    outputs = [attend(query_heads, key_heads, value_heads, totals[0])]
    attended = jnp.stack(outputs, axis=0)
    local_rows = lax.all_to_all(attended, "sp", split_axis=1, concat_axis=2, tiled=True)
    flat_rows = local_rows.reshape(-1, local_rows.shape[2])
    mixed = jnp.dot(
        flat_rows,
        lax.all_gather(w_out, "dp", axis=1, tiled=True),
        preferred_element_type=jnp.float32,
    )
    return mixed.astype(jnp.bfloat16).reshape(local_rows.shape[0], local_rows.shape[1], -1)


def solution(mesh):
    placed = (
        P("dp", "sp", None),
        P("dp", "sp", None),
        P("dp", "sp", None),
        P("dp", "sp", None),
        P(None, "dp"),
    )
    return jax.shard_map(
        local, mesh=mesh, in_specs=placed, out_specs=P("dp", "sp", None), check_vma=False
    )
```

profile of v0, /device:TPU:0, one launch (start us, length us, event | category | flops | bytes accessed | tf_op | source)
XLA Modules:
  0.0 138.5 jit_solution(7458643636415226542)
XLA Ops:
  6.5 0.7 all-gather.2.cloned.1.call-update
  7.3 7.3 %all-to-all-start.2 = ((f32[1,128,32]{1,0,2:T(1,128)}), f32[1,128,32]{1,0,2:T(1,128)S(1)}, u32[]{:S(2)}, u32[]{:S(2)}) async-start(f32[1,128,32]{1,0,2:T(1,128)} %bitcast.98), calls=%async_computation.2 | async-start | bytes 32768 | tf_op jit(solution)/shard_map/all_to_all | solution.py:45
  14.6 2.3 %copy.32 = bf16[1,128,2048]{1,0,2:T(2,128)(2,1)S(1)} copy(bf16[1,128,2048]{2,1,0:T(8,128)(2,1)} %param.6) | data formatting | bytes 1048576 | tf_op args[1]
  16.9 0.6 broadcast.36
  17.5 11.6 %reduce.2 = bf16[2048,128]{1,0:T(8,128)(2,1)S(1)} reduce(bf16[2048,1,128]{2,1,0:T(2,128)(2,1)S(1)} %bitcast.83, bf16[]{:T(256)} %broadcast.36), dimensions={1}, to_apply=%bitcast.66.reduce_sub_computation | reduce | bytes 1048578
  29.0 1.0 reshape.70
  30.0 6.0 %all-to-all-start.1 = ((bf16[8,2,16384]{2,1,0:T(2,128)(2,1)}), bf16[8,2,16384]{2,1,0:T(2,128)(2,1)S(1)}, u32[]{:S(2)}, u32[]{:S(2)}) async-start(bf16[8,2,16384]{2,1,0:T(2,128)(2,1)} %reshape.70), calls=%async_computation.1 | async-start | bytes 1048576 | tf_op jit(solution)/shard_map/all_to_all | solution.py:42
  36.0 0.8 copy.35
  36.8 11.5 %reduce = bf16[2048,128]{1,0:T(8,128)(2,1)S(1)} reduce(bf16[2048,1,128]{2,1,0:T(2,128)(2,1)S(1)} %bitcast.85, bf16[]{:T(256)} %broadcast.36), dimensions={1}, to_apply=%bitcast.62.reduce_sub_computation | reduce | bytes 1048578
  48.3 0.9 reshape.66
  49.2 0.8 all-to-all-done.1
  50.0 5.2 %all-to-all-start.3 = ((bf16[8,2,16384]{2,1,0:T(2,128)(2,1)}), bf16[8,2,16384]{2,1,0:T(2,128)(2,1)S(1)}, u32[]{:S(2)}, u32[]{:S(2)}) async-start(bf16[8,2,16384]{2,1,0:T(2,128)(2,1)} %reshape.66), calls=%async_computation.3 | async-start | bytes 1048576 | tf_op jit(solution)/shard_map/all_to_all | solution.py:43
  55.2 0.8 copy.30
  56.0 11.5 %reduce.1 = bf16[2048,128]{1,0:T(8,128)(2,1)S(1)} reduce(bf16[2048,1,128]{2,1,0:T(2,128)(2,1)S(1)} %bitcast.86, bf16[]{:T(256)} %broadcast.36), dimensions={1}, to_apply=%bitcast.64.reduce_sub_computation | reduce | bytes 1048578
  67.5 1.0 reshape.68
  68.6 5.9 %all-to-all-start = ((bf16[8,2,16384]{2,1,0:T(2,128)(2,1)}), bf16[8,2,16384]{2,1,0:T(2,128)(2,1)S(1)}, u32[]{:S(2)}, u32[]{:S(2)}) async-start(bf16[8,2,16384]{2,1,0:T(2,128)(2,1)} %reshape.68), calls=%async_computation | async-start | bytes 1048576 | tf_op jit(solution)/shard_map/all_to_all | solution.py:41
  74.9 0.5 reshape.71
  75.9 0.7 slice.45
  77.6 0.7 slice.43
  78.3 8.9 %all-to-all-done = bf16[8,2,16384]{2,1,0:T(2,128)(2,1)S(1)} async-done(((bf16[8,2,16384]{2,1,0:T(2,128)(2,1)}), bf16[8,2,16384]{2,1,0:T(2,128)(2,1)S(1)}, u32[]{:S(2)}, u32[]{:S(2)}) %all-to-all-start) | async-done | bytes 524320 | tf_op jit(solution)/shard_map/all_to_all | solution.py:41
  88.1 0.8 mul.15
  89.0 1.0 reshape_squeeze.7
  91.2 1.2 fusion.8
  92.3 1.2 fusion.6
  93.6 1.4 %fusion.22 = bf16[512,4,64]{0,2,1:T(8,128)(2,1)S(1)} fusion(bf16[512,4,64]{0,2,1:T(8,128)(2,1)S(1)} %slice.39, f32[4,512,512]{1,2,0:T(8,128)S(1)} %get-tuple-element.12, f32[4,512]{1,0:T(4,128)S(1)} %get-tuple-element.11, f32[4,512]{1,0:T(4,128)S(1)} %get-tuple-element.7, pred[512,512]{0,1:T(8,128)(4,1)S(1)} %iota_compare_fusion.1, f32[512,4]{0,1:T(4,128)S(1)} %bitcast.100), kind=kOutput, calls=%fused_computation.21 | convolution fusion | flops 139722752 | bytes 5005312 | tf_op jit(solution)/shard_map/hqk,khd->qhd/dot_general | solution.py:31
  95.1 2.2 %fusion.2 = (f32[4,512]{1,0:T(4,128)S(1)}, f32[4,512,1024]{2,1,0:T(8,128)S(1)}) fusion(f32[4,1024]{1,0:T(4,128)S(1)} %bitcast.95, f32[4,512]{1,0:T(4,128)S(1)} %get-tuple-element.8, pred[512,1024]{1,0:T(8,128)(4,1)S(1)} %iota_compare_fusion, bf16[512,4,64]{0,2,1:T(8,128)(2,1)S(1)} %copy-done.5, bf16[1024,4,64]{0,2,1:T(8,128)(2,1)S(1)} %copy-done.4), kind=kOutput, calls=%fused_computation.4 | convolution fusion | flops 276822016 | bytes 9732096 | tf_op jit(solution)/shard_map/qhd,khd->hqk/dot_general | solution.py:16
  97.3 2.8 %fusion = f32[4,512]{1,0:T(4,128)S(1)} fusion(f32[4,512,1024]{2,1,0:T(8,128)S(1)} %get-tuple-element.10, f32[4,512]{1,0:T(4,128)S(1)} %get-tuple-element.9, f32[4,1024]{1,0:T(4,128)S(1)} %bitcast.96, f32[4,512]{1,0:T(4,128)S(1)} %get-tuple-element.8, pred[512,1024]{1,0:T(8,128)(4,1)S(1)} %iota_compare_fusion), kind=kLoop, calls=%fused_computation.2 | loop fusion | flops 10483712 | bytes 8953856 | tf_op jit(solution)/shard_map/reduce_sum | solution.py:29
  100.1 2.8 %fusion.28 = bf16[512,4,64]{0,2,1:T(8,128)(2,1)S(1)} fusion(bf16[1024,4,64]{0,2,1:T(8,128)(2,1)S(1)} %reshape_squeeze.8, f32[4,512,1024]{2,1,0:T(8,128)S(1)} %get-tuple-element.10, f32[4,512]{1,0:T(4,128)S(1)} %get-tuple-element.9, f32[4,1024]{1,0:T(4,128)S(1)} %bitcast.97, f32[4,512]{1,0:T(4,128)S(1)} %get-tuple-element.8, ...), kind=kOutput, calls=%fused_computation.23 | convolution fusion | flops 279183360 | bytes 9740288 | tf_op jit(solution)/shard_map/hqk,khd->qhd/dot_general | solution.py:31
  103.0 1.1 copy.41
  104.1 3.8 %reduce.3 = bf16[1024,256]{1,0:T(8,128)(2,1)S(1)} reduce(bf16[1024,1,256]{2,1,0:T(2,128)(2,1)S(1)} %bitcast.84, bf16[]{:T(256)} %broadcast.36), dimensions={1}, to_apply=%bitcast.68.reduce_sub_computation | reduce | bytes 1048578
  108.0 17.2 %all_to_all.75 = bf16[8,2,16384]{2,1,0:T(2,128)(2,1)S(1)} all-to-all(bf16[8,2,16384]{2,1,0:T(2,128)(2,1)S(1)} %reshape.72), channel_id=1, replica_groups=mesh['sp'=8,'dp'=4] {'sp'}, dimensions={0} | all-to-all | bytes 1048576 | tf_op jit(solution)/shard_map/all_to_all | solution.py:52
  126.2 5.5 %fusion.9 = bf16[1,128,2048]{2,1,0:T(8,128)(2,1)} fusion(bf16[128,2048]{0,1:T(8,128)(2,1)S(1)} %bitcast.78, bf16[2048,2048]{1,0:T(8,128)(2,1)} %all-gather.2.cloned.1.call-done), kind=kOutput, calls=%fused_computation.13 | convolution fusion | flops 1074003968 | bytes 9437184 | tf_op jit(solution)/shard_map/dot_general | solution.py:54
  (41 shorter events, 5.0 us)
Async XLA Ops:
  6.5 29.5 %copy-start.2 = (bf16[1,128,2048]{2,1,0:T(8,128)(2,1)S(1)}, bf16[1,128,2048]{2,1,0:T(8,128)(2,1)}, u32[]{:S(2)}) copy-start(bf16[1,128,2048]{2,1,0:T(8,128)(2,1)} %param.7) | copy-start | bytes 1572868
  6.5 119.6 %all-gather.2.cloned.1.call-start = ((), (), s32[]{:S(2)}) async-start(), calls=%async_computation.5 | async-start | bytes 10485760 | tf_op jit(solution)/shard_map/all_gather | solution.py:56
  7.3 22.8 %all-to-all-start.2 = ((f32[1,128,32]{1,0,2:T(1,128)}), f32[1,128,32]{1,0,2:T(1,128)S(1)}, u32[]{:S(2)}, u32[]{:S(2)}) async-start(f32[1,128,32]{1,0,2:T(1,128)} %bitcast.98), calls=%async_computation.2 | async-start | bytes 32768 | tf_op jit(solution)/shard_map/all_to_all | solution.py:45
  17.5 37.7 %copy-start.3 = (bf16[1,128,2048]{2,1,0:T(8,128)(2,1)S(1)}, bf16[1,128,2048]{2,1,0:T(8,128)(2,1)}, u32[]{:S(2)}) copy-start(bf16[1,128,2048]{2,1,0:T(8,128)(2,1)} %param.5) | copy-start | bytes 1572868
  30.0 20.0 %all-to-all-start.1 = ((bf16[8,2,16384]{2,1,0:T(2,128)(2,1)}), bf16[8,2,16384]{2,1,0:T(2,128)(2,1)S(1)}, u32[]{:S(2)}, u32[]{:S(2)}) async-start(bf16[8,2,16384]{2,1,0:T(2,128)(2,1)} %reshape.70), calls=%async_computation.1 | async-start | bytes 1048576 | tf_op jit(solution)/shard_map/all_to_all | solution.py:42
  50.0 18.6 %all-to-all-start.3 = ((bf16[8,2,16384]{2,1,0:T(2,128)(2,1)}), bf16[8,2,16384]{2,1,0:T(2,128)(2,1)S(1)}, u32[]{:S(2)}, u32[]{:S(2)}) async-start(bf16[8,2,16384]{2,1,0:T(2,128)(2,1)} %reshape.66), calls=%async_computation.3 | async-start | bytes 1048576 | tf_op jit(solution)/shard_map/all_to_all | solution.py:43
  68.6 18.7 %all-to-all-start = ((bf16[8,2,16384]{2,1,0:T(2,128)(2,1)}), bf16[8,2,16384]{2,1,0:T(2,128)(2,1)S(1)}, u32[]{:S(2)}, u32[]{:S(2)}) async-start(bf16[8,2,16384]{2,1,0:T(2,128)(2,1)} %reshape.68), calls=%async_computation | async-start | bytes 1048576 | tf_op jit(solution)/shard_map/all_to_all | solution.py:41
  87.8 2.7 %copy-start = (bf16[1,4,128,256]{2,3,1,0:T(8,128)(2,1)S(1)}, bf16[1,4,128,256]{2,3,1,0:T(8,128)(2,1)}, u32[]{:S(2)}) copy-start(bf16[1,4,128,256]{2,3,1,0:T(8,128)(2,1)} %slice.45) | copy-start | bytes 786436
  87.8 3.1 %copy-start.1 = (bf16[1,4,128,256]{2,3,1,0:T(8,128)(2,1)S(1)}, bf16[1,4,128,256]{2,3,1,0:T(8,128)(2,1)}, u32[]{:S(2)}) copy-start(bf16[1,4,128,256]{2,3,1,0:T(8,128)(2,1)} %slice.43) | copy-start | bytes 786436
  93.6 1.5 %copy-start.4 = (bf16[1024,4,64]{0,2,1:T(8,128)(2,1)S(1)}, bf16[1024,4,64]{0,2,1:T(8,128)(2,1)}, u32[]{:S(2)}) copy-start(bf16[1024,4,64]{0,2,1:T(8,128)(2,1)} %reshape_squeeze.7) | copy-start | bytes 1572868
  93.6 1.5 %copy-start.5 = (bf16[512,4,64]{0,2,1:T(8,128)(2,1)S(1)}, bf16[512,4,64]{0,2,1:T(8,128)(2,1)}, u32[]{:S(2)}) copy-start(bf16[512,4,64]{0,2,1:T(8,128)(2,1)} %mul.15) | copy-start | bytes 786436
Sparse Core Ops, SparseCore 0:
  8.9 60.9 all-gather.1
where the time goes:
time: 139 us; the launch traced here: 138 us
  other arithmetic  43 us (31%)
  starting transfers between devices  24.4 us (18%)
  blocking collectives  17.2 us (12%)
  local copies, waits for them, and re-layouts  16.5 us (12%)
  between operations  13.7 us (10%)
  matrix products  13.1 us (9%)
  waiting for transfers between devices  10.5 us (8%)
    unnamed x4, other arithmetic  38.4 us
    all_to_all x1, blocking collectives, local(): lax.all_to_all(attended, 'sp', split_axis=1, concat_axis=2, tiled=True)  17.2 us
    unnamed x28, local copies, waits for them, and re-layouts  9.83 us
    all_to_all x1, waiting for transfers between devices, local(): lax.all_to_all(queries, 'sp', split_axis=2, concat_axis=1, tiled=True)  8.91 us
    all_to_all x1, starting transfers between devices, local(): lax.all_to_all(gate_totals, 'sp', split_axis=2, concat_axis=1, tiled=True)  7.29 us
    all_to_all x1, starting transfers between devices, local(): lax.all_to_all(keys, 'sp', split_axis=2, concat_axis=1, tiled=True)  6 us
    all_to_all x1, starting transfers between devices, local(): lax.all_to_all(queries, 'sp', split_axis=2, concat_axis=1, tiled=True)  5.88 us
    dot_general x1, matrix products, local(): jnp.dot(flat_rows, lax.all_gather(w_out, 'dp', axis=1, tiled=True), prefe...  5.46 us
  transfers between devices with their start and end apart: 5, of which 3 were waited for; matrix products, arithmetic and copies ran while one was open for 48% of the time, Pallas kernels for 0%

commit v1 on v0

--- a/solution.py
+++ b/solution.py
@@ -49,7 +49,10 @@
     ]
     outputs = [attend(query_heads, key_heads, value_heads, totals[0])]
     attended = jnp.stack(outputs, axis=0)
-    local_rows = lax.all_to_all(attended, "sp", split_axis=1, concat_axis=2, tiled=True)
+    local_rows = jnp.concatenate(
+        lax.all_to_all(jnp.stack(jnp.split(attended, lax.axis_size("sp"), axis=1)), "sp", 0, 0),
+        axis=2,
+    )
     flat_rows = local_rows.reshape(-1, local_rows.shape[2])
     mixed = jnp.dot(
         flat_rows,

time: 139 us -> 133 us (0.957)
  other arithmetic: 43 us -> 39.2 us
  local copies, waits for them, and re-layouts: 16.5 us -> 14.7 us
    unnamed x4 -> x3, other arithmetic: 38.4 us -> 34.6 us
    unnamed x28 -> x32, local copies, waits for them, and re-layouts: 9.83 us -> 9.31 us
  transfers between devices with their start and end apart: 5 -> 5, of which waited for: 3 -> 3; matrix products, arithmetic and copies ran while one was open for 48% -> 46% of each run, Pallas kernels for 0% -> 0%
where the time goes in v1:
time: 133 us
  other arithmetic  39.2 us (29%)
  starting transfers between devices  24.4 us (18%)
  blocking collectives  17.2 us (13%)
  local copies, waits for them, and re-layouts  14.7 us (11%)
  between operations  13.7 us (10%)
  matrix products  13.1 us (10%)
  waiting for transfers between devices  10.5 us (8%)
    unnamed x3, other arithmetic  34.6 us
    all_to_all x1, blocking collectives, local(): lax.all_to_all(jnp.stack(jnp.split(attended, lax.axis_size('sp'), axis=1)...  17.2 us
    unnamed x32, local copies, waits for them, and re-layouts  9.31 us
    all_to_all x1, waiting for transfers between devices, local(): lax.all_to_all(queries, 'sp', split_axis=2, concat_axis=1, tiled=True)  8.91 us
    all_to_all x1, starting transfers between devices, local(): lax.all_to_all(gate_totals, 'sp', split_axis=2, concat_axis=1, tiled=True)  7.29 us
    all_to_all x1, starting transfers between devices, local(): lax.all_to_all(keys, 'sp', split_axis=2, concat_axis=1, tiled=True)  6 us
    all_to_all x1, starting transfers between devices, local(): lax.all_to_all(queries, 'sp', split_axis=2, concat_axis=1, tiled=True)  5.88 us
    dot_general x1, matrix products, local(): jnp.dot(flat_rows, lax.all_gather(w_out, 'dp', axis=1, tiled=True), prefe...  5.46 us
  transfers between devices with their start and end apart: 5, of which 3 were waited for; matrix products, arithmetic and copies ran while one was open for 46% of the time, Pallas kernels for 0%

profile of v1, /device:TPU:0, one launch (start us, length us, event | category | flops | bytes accessed | tf_op | source)
XLA Modules:
  0.0 132.8 jit_solution(10239288332971865691)
XLA Ops:
  6.5 0.7 all-gather.2.cloned.1.call-update
  7.3 7.3 %all-to-all-start.2 = ((f32[1,128,32]{1,0,2:T(1,128)}), f32[1,128,32]{1,0,2:T(1,128)S(1)}, u32[]{:S(2)}, u32[]{:S(2)}) async-start(f32[1,128,32]{1,0,2:T(1,128)} %bitcast.131), calls=%async_computation.2 | async-start | bytes 32768 | tf_op jit(solution)/shard_map/all_to_all | solution.py:45
  14.6 2.3 %copy.20 = bf16[1,128,2048]{1,0,2:T(2,128)(2,1)S(1)} copy(bf16[1,128,2048]{2,1,0:T(8,128)(2,1)} %param.6) | data formatting | bytes 1048576 | tf_op args[1]
  16.9 0.6 broadcast.36
  17.5 11.6 %reduce.2 = bf16[2048,128]{1,0:T(8,128)(2,1)S(1)} reduce(bf16[2048,1,128]{2,1,0:T(2,128)(2,1)S(1)} %bitcast.111, bf16[]{:T(256)} %broadcast.36), dimensions={1}, to_apply=%bitcast.97.reduce_sub_computation | reduce | bytes 1048578
  29.0 1.0 reshape.69
  30.0 6.0 %all-to-all-start.1 = ((bf16[8,2,16384]{2,1,0:T(2,128)(2,1)}), bf16[8,2,16384]{2,1,0:T(2,128)(2,1)S(1)}, u32[]{:S(2)}, u32[]{:S(2)}) async-start(bf16[8,2,16384]{2,1,0:T(2,128)(2,1)} %reshape.69), calls=%async_computation.1 | async-start | bytes 1048576 | tf_op jit(solution)/shard_map/all_to_all | solution.py:42
  36.0 0.8 copy.23
  36.8 11.5 %reduce = bf16[2048,128]{1,0:T(8,128)(2,1)S(1)} reduce(bf16[2048,1,128]{2,1,0:T(2,128)(2,1)S(1)} %bitcast.113, bf16[]{:T(256)} %broadcast.36), dimensions={1}, to_apply=%bitcast.93.reduce_sub_computation | reduce | bytes 1048578
  48.3 0.9 reshape.65
  49.2 0.8 all-to-all-done.1
  50.0 5.2 %all-to-all-start.3 = ((bf16[8,2,16384]{2,1,0:T(2,128)(2,1)}), bf16[8,2,16384]{2,1,0:T(2,128)(2,1)S(1)}, u32[]{:S(2)}, u32[]{:S(2)}) async-start(bf16[8,2,16384]{2,1,0:T(2,128)(2,1)} %reshape.65), calls=%async_computation.3 | async-start | bytes 1048576 | tf_op jit(solution)/shard_map/all_to_all | solution.py:43
  55.2 0.8 copy.18
  56.0 11.5 %reduce.1 = bf16[2048,128]{1,0:T(8,128)(2,1)S(1)} reduce(bf16[2048,1,128]{2,1,0:T(2,128)(2,1)S(1)} %bitcast.112, bf16[]{:T(256)} %broadcast.36), dimensions={1}, to_apply=%bitcast.95.reduce_sub_computation | reduce | bytes 1048578
  67.5 1.0 reshape.67
  68.6 5.9 %all-to-all-start = ((bf16[8,2,16384]{2,1,0:T(2,128)(2,1)}), bf16[8,2,16384]{2,1,0:T(2,128)(2,1)S(1)}, u32[]{:S(2)}, u32[]{:S(2)}) async-start(bf16[8,2,16384]{2,1,0:T(2,128)(2,1)} %reshape.67), calls=%async_computation | async-start | bytes 1048576 | tf_op jit(solution)/shard_map/all_to_all | solution.py:41
  74.9 0.5 reshape.70
  75.9 0.7 slice.45
  76.6 0.5 reshape.66
  77.6 0.7 slice.43
  78.3 8.9 %all-to-all-done = bf16[8,2,16384]{2,1,0:T(2,128)(2,1)S(1)} async-done(((bf16[8,2,16384]{2,1,0:T(2,128)(2,1)}), bf16[8,2,16384]{2,1,0:T(2,128)(2,1)S(1)}, u32[]{:S(2)}, u32[]{:S(2)}) %all-to-all-start) | async-done | bytes 524320 | tf_op jit(solution)/shard_map/all_to_all | solution.py:41
  87.2 0.5 reshape.68
  88.1 0.8 mul.15
  89.0 1.0 reshape_squeeze.7
  91.2 1.2 fusion.8
  92.4 1.2 fusion.6
  93.6 1.4 %fusion.22 = bf16[512,4,64]{0,2,1:T(8,128)(2,1)S(1)} fusion(bf16[512,4,64]{0,2,1:T(8,128)(2,1)S(1)} %slice.39, f32[4,512,512]{1,2,0:T(8,128)S(1)} %get-tuple-element.12, f32[4,512]{1,0:T(4,128)S(1)} %get-tuple-element.11, f32[4,512]{1,0:T(4,128)S(1)} %get-tuple-element.7, pred[512,512]{0,1:T(8,128)(4,1)S(1)} %iota_compare_fusion.1, f32[512,4]{0,1:T(4,128)S(1)} %bitcast.133), kind=kOutput, calls=%fused_computation.21 | convolution fusion | flops 139722752 | bytes 5005312 | tf_op jit(solution)/shard_map/hqk,khd->qhd/dot_general | solution.py:31
  95.1 2.2 %fusion.2 = (f32[4,512]{1,0:T(4,128)S(1)}, f32[4,512,1024]{2,1,0:T(8,128)S(1)}) fusion(f32[4,1024]{1,0:T(4,128)S(1)} %bitcast.128, f32[4,512]{1,0:T(4,128)S(1)} %get-tuple-element.8, pred[512,1024]{1,0:T(8,128)(4,1)S(1)} %iota_compare_fusion, bf16[512,4,64]{0,2,1:T(8,128)(2,1)S(1)} %copy-done.5, bf16[1024,4,64]{0,2,1:T(8,128)(2,1)S(1)} %copy-done.4), kind=kOutput, calls=%fused_computation.4 | convolution fusion | flops 276822016 | bytes 9732096 | tf_op jit(solution)/shard_map/qhd,khd->hqk/dot_general | solution.py:16
  97.3 2.8 %fusion = f32[4,512]{1,0:T(4,128)S(1)} fusion(f32[4,512,1024]{2,1,0:T(8,128)S(1)} %get-tuple-element.10, f32[4,512]{1,0:T(4,128)S(1)} %get-tuple-element.9, f32[4,1024]{1,0:T(4,128)S(1)} %bitcast.129, f32[4,512]{1,0:T(4,128)S(1)} %get-tuple-element.8, pred[512,1024]{1,0:T(8,128)(4,1)S(1)} %iota_compare_fusion), kind=kLoop, calls=%fused_computation.2 | loop fusion | flops 10483712 | bytes 8953856 | tf_op jit(solution)/shard_map/reduce_sum | solution.py:29
  100.2 2.8 %fusion.28 = bf16[512,4,64]{0,2,1:T(8,128)(2,1)S(1)} fusion(bf16[1024,4,64]{0,2,1:T(8,128)(2,1)S(1)} %reshape_squeeze.8, f32[4,512,1024]{2,1,0:T(8,128)S(1)} %get-tuple-element.10, f32[4,512]{1,0:T(4,128)S(1)} %get-tuple-element.9, f32[4,1024]{1,0:T(4,128)S(1)} %bitcast.130, f32[4,512]{1,0:T(4,128)S(1)} %get-tuple-element.8, ...), kind=kOutput, calls=%fused_computation.23 | convolution fusion | flops 279183360 | bytes 9740288 | tf_op jit(solution)/shard_map/hqk,khd->qhd/dot_general | solution.py:31
  103.3 17.2 %all_to_all.65 = bf16[8,1,128,256]{2,3,1,0:T(8,128)(2,1)S(1)} all-to-all(bf16[8,1,128,256]{2,3,1,0:T(8,128)(2,1)S(1)} %fusion.31), channel_id=1, replica_groups=mesh['sp'=8,'dp'=4] {'sp'}, dimensions={0} | all-to-all | bytes 1048576 | tf_op jit(solution)/shard_map/all_to_all | solution.py:53
  120.5 5.5 %fusion.9 = bf16[1,128,2048]{2,1,0:T(8,128)(2,1)} fusion(bf16[128,2048]{0,1:T(8,128)(2,1)S(1)} %bitcast.107, bf16[2048,2048]{1,0:T(8,128)(2,1)} %all-gather.2.cloned.1.call-done), kind=kOutput, calls=%fused_computation.13 | convolution fusion | flops 1074003968 | bytes 9437184 | tf_op jit(solution)/shard_map/dot_general | solution.py:57
  (43 shorter events, 3.2 us)
Async XLA Ops:
  6.5 29.5 %copy-start.2 = (bf16[1,128,2048]{2,1,0:T(8,128)(2,1)S(1)}, bf16[1,128,2048]{2,1,0:T(8,128)(2,1)}, u32[]{:S(2)}) copy-start(bf16[1,128,2048]{2,1,0:T(8,128)(2,1)} %param.7) | copy-start | bytes 1572868
  6.5 114.0 %all-gather.2.cloned.1.call-start = ((), (), s32[]{:S(2)}) async-start(), calls=%async_computation.5 | async-start | bytes 10485760 | tf_op jit(solution)/shard_map/all_gather | solution.py:59
  7.3 22.8 %all-to-all-start.2 = ((f32[1,128,32]{1,0,2:T(1,128)}), f32[1,128,32]{1,0,2:T(1,128)S(1)}, u32[]{:S(2)}, u32[]{:S(2)}) async-start(f32[1,128,32]{1,0,2:T(1,128)} %bitcast.131), calls=%async_computation.2 | async-start | bytes 32768 | tf_op jit(solution)/shard_map/all_to_all | solution.py:45
  17.5 37.7 %copy-start.3 = (bf16[1,128,2048]{2,1,0:T(8,128)(2,1)S(1)}, bf16[1,128,2048]{2,1,0:T(8,128)(2,1)}, u32[]{:S(2)}) copy-start(bf16[1,128,2048]{2,1,0:T(8,128)(2,1)} %param.5) | copy-start | bytes 1572868
  30.0 20.0 %all-to-all-start.1 = ((bf16[8,2,16384]{2,1,0:T(2,128)(2,1)}), bf16[8,2,16384]{2,1,0:T(2,128)(2,1)S(1)}, u32[]{:S(2)}, u32[]{:S(2)}) async-start(bf16[8,2,16384]{2,1,0:T(2,128)(2,1)} %reshape.69), calls=%async_computation.1 | async-start | bytes 1048576 | tf_op jit(solution)/shard_map/all_to_all | solution.py:42
  50.0 18.6 %all-to-all-start.3 = ((bf16[8,2,16384]{2,1,0:T(2,128)(2,1)}), bf16[8,2,16384]{2,1,0:T(2,128)(2,1)S(1)}, u32[]{:S(2)}, u32[]{:S(2)}) async-start(bf16[8,2,16384]{2,1,0:T(2,128)(2,1)} %reshape.65), calls=%async_computation.3 | async-start | bytes 1048576 | tf_op jit(solution)/shard_map/all_to_all | solution.py:43
  68.6 18.7 %all-to-all-start = ((bf16[8,2,16384]{2,1,0:T(2,128)(2,1)}), bf16[8,2,16384]{2,1,0:T(2,128)(2,1)S(1)}, u32[]{:S(2)}, u32[]{:S(2)}) async-start(bf16[8,2,16384]{2,1,0:T(2,128)(2,1)} %reshape.67), calls=%async_computation | async-start | bytes 1048576 | tf_op jit(solution)/shard_map/all_to_all | solution.py:41
  87.8 2.8 %copy-start = (bf16[1,4,128,256]{2,3,1,0:T(8,128)(2,1)S(1)}, bf16[1,4,128,256]{2,3,1,0:T(8,128)(2,1)}, u32[]{:S(2)}) copy-start(bf16[1,4,128,256]{2,3,1,0:T(8,128)(2,1)} %slice.45) | copy-start | bytes 786436
  87.8 3.1 %copy-start.1 = (bf16[1,4,128,256]{2,3,1,0:T(8,128)(2,1)S(1)}, bf16[1,4,128,256]{2,3,1,0:T(8,128)(2,1)}, u32[]{:S(2)}) copy-start(bf16[1,4,128,256]{2,3,1,0:T(8,128)(2,1)} %slice.43) | copy-start | bytes 786436
  93.6 1.5 %copy-start.4 = (bf16[1024,4,64]{0,2,1:T(8,128)(2,1)S(1)}, bf16[1024,4,64]{0,2,1:T(8,128)(2,1)}, u32[]{:S(2)}) copy-start(bf16[1024,4,64]{0,2,1:T(8,128)(2,1)} %reshape_squeeze.7) | copy-start | bytes 1572868
  93.6 1.5 %copy-start.5 = (bf16[512,4,64]{0,2,1:T(8,128)(2,1)S(1)}, bf16[512,4,64]{0,2,1:T(8,128)(2,1)}, u32[]{:S(2)}) copy-start(bf16[512,4,64]{0,2,1:T(8,128)(2,1)} %mul.15) | copy-start | bytes 786436
Sparse Core Ops, SparseCore 0:
  8.9 60.9 all-gather.1
